TPU v7x, 512 devices: a 4x2x32 block of a 4x8x32 slice. The times are simulated.
512 devices in a mesh: grp: 2 (over y), sp: 32 (over z), tp: 8 (over x, core).
Axes of the slice: x: 4, y: 2, z: 32, core: 2. Of those that a mesh axis runs over, the one named last changes fastest.
The devices are a block of a 4x8x32 slice.
Arguments:
- tokens_in: bfloat16 [16384, 2048], P(('grp', 'sp')), parts along dimension 0, may hold values from -6 to 6
- input_gain: float32 [2048], replicated, may hold values from 0.1 to 1.9
- w_query: bfloat16 [2048, 1024], P('sp', 'tp'), may hold values from -0.125 to 0.125
- w_key: bfloat16 [2048, 1024], P('sp', 'tp'), may hold values from -1 to 1
- w_value: bfloat16 [2048, 1024], P('sp', 'tp'), may hold values from -0.125 to 0.125
- w_gates: bfloat16 [2048, 32], P('sp', 'tp'), may hold values from -3 to 3
- w_glu_value: bfloat16 [2048, 1024], P('sp', 'tp'), may hold values from -0.125 to 0.125
- sigmoid_opener_matrix: bfloat16 [2048, 1024], P('sp', 'tp'), may hold values from -0.125 to 0.125
- log_decay: float32 [16384, 16], P(('grp', 'sp'), 'tp'), parts along dimension 0, may hold values from -1 to 0
- head_gain: float32 [128], replicated, may hold values from 0.1 to 1.9
- conv_kernel: float32 [31, 1024], P(None, 'tp'), may hold values from -12 to 12
- norm_gain: float32 [1024], P('tp'), may hold values from 0.1 to 1.9
- norm_shift: float32 [1024], P('tp'), may hold values from -3 to 3
- out_delta: bfloat16 [2048, 1024], P(None, 'tp'), may hold values from -0.125 to 0.125
- out_conv: bfloat16 [2048, 1024], P(None, 'tp'), may hold values from -0.125 to 0.125
Outputs:
- mixed: bfloat16 [16384, 2048], P(('grp', 'sp'), 'tp'), parts along dimension 0
There are 2 independent parts, one for each index of `grp`. A program takes and returns all parts, laid end to end along the dimension named above; an argument that names none is the same for every part. Nothing has to cross between parts.
All inputs are finite; a program needn't handle non-finite values.
Results may differ from a plain program's by a relative error of at most 0.015.
Values may be sent and summed in bfloat16 or wider, within the bound.
A program may use at most 64 MiB of HBM per device.

v0:
```python
import jax
import jax.numpy as jnp
from jax import lax
from jax.sharding import PartitionSpec as P

CONV_CH = 1024
BLOCK = 64


PRECISE = lax.Precision.HIGHEST
EPSILON = 1e-06
BETA_SHIFT = 6.0


def from_everyone(value, axis):
    copies = jnp.broadcast_to(value, (lax.axis_size(axis), *value.shape))
    return lax.all_to_all(copies, axis, split_axis=0, concat_axis=0, tiled=True)


def folded_in_pairs(pieces, combine):
    while len(jax.tree.leaves(pieces)[0]) > 1:
        pieces = jax.vmap(combine)(
            *(jax.tree.map(lambda part: part[side::2], pieces) for side in (0, 1))
        )
    return jax.tree.map(lambda part: part[0], pieces)


def entering(value, axis, combine, identity):
    devices, place = (lax.axis_size(axis), lax.axis_index(axis))
    passed = jnp.arange(devices) < place

    def kept(part, zero, own):
        part = jnp.where(
            passed.reshape(-1, *(1 for _ in own.shape)),
            part.astype(own.dtype),
            jnp.asarray(zero, own.dtype),
        )
        return part

    pieces = jax.tree.map(
        lambda part: from_everyone(part, axis),
        jax.tree.map(lambda part, kind: part.astype(kind), value, (jnp.bfloat16, jnp.bfloat16)),
    )
    return folded_in_pairs(jax.tree.map(kept, pieces, identity, value), combine)


def entering_2(value, axis, combine, identity):
    devices, place = (lax.axis_size(axis), lax.axis_index(axis))
    everything = jax.tree.map(
        lambda part, kind: lax.all_gather(part.astype(kind), axis),
        value,
        (jnp.bfloat16, jnp.bfloat16),
    )
    start = jax.tree.map(
        lambda part, zero: jnp.broadcast_to(jnp.asarray(zero, part.dtype), part.shape),
        value,
        identity,
    )

    def lap(k, before):
        at = devices - 1 - k
        reached = at > place
        new = combine(
            before, jax.tree.map(lambda part, own: part[at].astype(own.dtype), everything, value)
        )
        return jax.tree.map(lambda a, b: jnp.where(reached, a, b), new, before)

    return lax.fori_loop(0, devices, lap, start)


def with_halo(block, sides, width):
    for axis, dim in sides:
        count = lax.axis_size(axis)
        forward = [(i, i + 1) for i in range(count - 1)]
        backward = [(target, source) for source, target in forward]
        low = lax.ppermute(
            lax.slice_in_dim(block, block.shape[dim] - width, None, axis=dim), axis, forward
        )
        high = lax.ppermute(lax.slice_in_dim(block, 0, width, axis=dim), axis, backward)
        block = jnp.concatenate([low, block, high], axis=dim)
    return block


def of_everyone(value, axis):
    everything = from_everyone(value, axis)
    return jnp.sum(everything, axis=0)


def together(arrays, axis):
    flat, at, gathered = (jnp.concatenate([a.reshape(-1) for a in arrays]), 0, [])
    running = of_everyone(flat, axis)
    for a in arrays:
        gathered.append(running[at : at + a.size].reshape(a.shape))
        at += a.size
    return tuple(gathered)


def side_by_side(arrays, axis, dim, along):
    ends, at = ([], 0)
    for a in arrays[:-1]:
        at += a.shape[along]
        ends.append(at)
    both = jnp.concatenate(arrays, axis=along)
    return tuple(jnp.split(lax.all_gather(both, axis, axis=dim, tiled=True), ends, axis=along))


def split_up(value, dim, devices):
    shape = value.shape
    tiles = value.reshape(*shape[:dim], devices, shape[dim] // devices, *shape[dim + 1 :])
    return jnp.moveaxis(tiles, dim, 0)


def sum_at_owner(value, axis, dim):
    tiles = split_up(value, dim, lax.axis_size(axis))
    arrived = lax.all_to_all(tiles, axis, split_axis=0, concat_axis=0, tiled=True)
    return arrived.astype(jnp.float32).sum(axis=0)


def high_dot(left, right):
    return jnp.matmul(left, right, precision=PRECISE)


def swap_last(tensor):
    return jnp.swapaxes(tensor, -1, -2)


def block_terms(query, key_rows, values, decay_log, beta_rate, block):
    head_count, length = (query.shape[0], query.shape[1])
    blocks = length // block

    def to_blocks(tensor):
        return tensor.reshape((head_count, blocks, block) + tensor.shape[2:])

    query, key_rows, values, decay_log, beta_rate = (
        to_blocks(tensor) for tensor in (query, key_rows, values, decay_log, beta_rate)
    )
    cumulative = jnp.cumsum(decay_log, axis=-1)
    positions = jnp.arange(block)
    on_or_below = positions[:, None] >= positions[None, :]
    strict = positions[:, None] > positions[None, :]
    log_gaps = cumulative[..., :, None] - cumulative[..., None, :]
    weighting = jnp.where(on_or_below, jnp.exp(jnp.where(on_or_below, log_gaps, 0.0)), 0.0)
    scaled_keys = key_rows * beta_rate[..., None]
    lower_part = jnp.where(strict, high_dot(scaled_keys, swap_last(key_rows)) * weighting, 0.0)
    identity = jnp.eye(block, dtype=jnp.float32)
    inverse = jax.scipy.linalg.solve_triangular(
        identity + lower_part,
        jnp.broadcast_to(identity, lower_part.shape),
        lower=True,
        unit_diagonal=True,
    )
    update = high_dot(inverse, values * beta_rate[..., None])
    mixed_keys = high_dot(inverse, scaled_keys * jnp.exp(cumulative)[..., None])
    in_block = jnp.where(on_or_below, high_dot(query, swap_last(key_rows)) * weighting, 0.0)
    q_decayed = query * jnp.exp(cumulative)[..., None]
    k_decayed = key_rows * jnp.exp(cumulative[..., -1:] - cumulative)[..., None]
    end_decay = jnp.exp(cumulative[..., -1])
    return tuple(
        (
            jnp.moveaxis(tensor, 1, 0)
            for tensor in (update, mixed_keys, in_block, q_decayed, k_decayed, end_decay)
        )
    )


def delta_local(query, key_rows, values, decay_log, beta_rate):
    stacked = block_terms(query, key_rows, values, decay_log, beta_rate, BLOCK)
    head_count, length, head_width = query.shape
    identity = jnp.broadcast_to(
        jnp.eye(head_width, dtype=jnp.float32), (head_count, head_width, head_width)
    )
    zero_state = jnp.zeros((head_count, head_width, values.shape[2]), jnp.float32)

    def advance(carry, pieces):
        state_now, carried = carry
        update, mixed_keys, in_block, q_decayed, k_decayed, end_decay = pieces
        new_values = update - high_dot(mixed_keys, state_now)
        output = high_dot(q_decayed, state_now) + high_dot(in_block, new_values)
        reading = high_dot(q_decayed - high_dot(in_block, mixed_keys), carried)
        passing = end_decay[:, None, None] * identity - high_dot(swap_last(k_decayed), mixed_keys)
        state_now = state_now * end_decay[:, None, None] + high_dot(
            swap_last(k_decayed), new_values
        )
        return ((state_now, high_dot(passing, carried)), (output, reading))

    (state_now, carried), (output, reading) = lax.scan(advance, (zero_state, identity), stacked)
    output = jnp.moveaxis(output, 0, 1).reshape(head_count, length, values.shape[2])
    reading = jnp.moveaxis(reading, 0, 1).reshape(head_count, length, head_width)
    return (output, reading, carried, state_now)


def chain(earlier, later):
    return (high_dot(later[0], earlier[0]), high_dot(later[0], earlier[1]) + later[1])


def reversed_rows(tensor):
    return jnp.flip(tensor, axis=1)


def delta_branch(query_proj, key_proj, value_proj, gate_proj, log_decay, head_gain):
    head_width = head_gain.shape[0]
    length = query_proj.shape[0]
    head_count = query_proj.shape[1] // head_width

    def by_head(tensor):
        return jnp.swapaxes(jax.nn.silu(tensor).reshape(length, head_count, head_width), 0, 1)

    def unit_rows(tensor):
        return tensor * lax.rsqrt(jnp.sum(tensor * tensor, axis=-1, keepdims=True) + EPSILON)

    query = unit_rows(by_head(query_proj)) * head_width ** (-0.5)
    key_rows = unit_rows(by_head(key_proj))
    values = by_head(value_proj)
    gate_parts = gate_proj.reshape(length, head_count, 4)
    rate_parts = log_decay.reshape(length, head_count, 2)
    decay_fore = jnp.swapaxes(
        rate_parts[:, :, 0] * (0.5 + jax.nn.sigmoid(gate_parts[:, :, 0])), 0, 1
    )
    beta_fore = jnp.swapaxes(jax.nn.sigmoid(gate_parts[:, :, 1] - BETA_SHIFT), 0, 1)
    decay_back = jnp.swapaxes(
        rate_parts[:, :, 1] * (0.5 + jax.nn.sigmoid(gate_parts[:, :, 2])), 0, 1
    )
    beta_back = jnp.swapaxes(jax.nn.sigmoid(gate_parts[:, :, 3] - BETA_SHIFT), 0, 1)
    identity = jnp.broadcast_to(
        jnp.eye(head_width, dtype=jnp.float32), (head_count, head_width, head_width)
    )
    zero_state = jnp.zeros((head_count, head_width, head_width), jnp.float32)
    forward_out, forward_read, forward_map, forward_end = delta_local(
        query, key_rows, values, decay_fore, beta_fore
    )
    forward_start = entering((forward_map, forward_end), "sp", chain, (identity, zero_state))[1]
    back_out, back_read, back_map, back_end = delta_local(
        reversed_rows(query),
        reversed_rows(key_rows),
        reversed_rows(values),
        reversed_rows(decay_back),
        reversed_rows(beta_back),
    )
    back_start = entering_2((back_map, back_end), "sp", chain, (identity, zero_state))[1]
    joined = forward_out + high_dot(forward_read, forward_start)
    joined = joined + reversed_rows(back_out + high_dot(back_read, back_start))
    joined = (
        joined * lax.rsqrt(jnp.mean(joined * joined, axis=-1, keepdims=True) + EPSILON) * head_gain
    )
    return jnp.swapaxes(joined, 0, 1).reshape(length, head_count * head_width).astype(jnp.bfloat16)


def conv_branch(value_proj, gate_proj, conv_kernel, norm_gain, norm_shift):
    glu_rows = (value_proj * jax.nn.sigmoid(gate_proj)).astype(jnp.bfloat16)
    half_width = conv_kernel.shape[0] // 2
    length = glu_rows.shape[0]
    padded = with_halo(glu_rows, (("sp", 0),), half_width).astype(jnp.float32)
    conv_rows = padded[0:length] * conv_kernel[0]
    for offset in range(1, conv_kernel.shape[0]):
        conv_rows = conv_rows + padded[offset : offset + length] * conv_kernel[offset]
    row_sum, row_squares = together(
        (jnp.sum(conv_rows, axis=-1), jnp.sum(conv_rows * conv_rows, axis=-1)), "tp"
    )
    center = row_sum / CONV_CH
    spread = row_squares / CONV_CH - center * center
    normal_rows = (conv_rows - center[:, None]) * lax.rsqrt(spread + EPSILON)[:, None]
    return jax.nn.silu(normal_rows * norm_gain + norm_shift).astype(jnp.bfloat16)


def on_device(
    tokens_in,
    input_gain,
    w_query,
    w_key,
    w_value,
    w_gates,
    w_glu_value,
    sigmoid_opener_matrix,
    log_decay,
    head_gain,
    conv_kernel,
    norm_gain,
    norm_shift,
    out_delta,
    out_conv,
):
    rows = tokens_in.astype(jnp.float32)
    normed = (
        rows * lax.rsqrt(jnp.mean(rows * rows, axis=-1, keepdims=True) + EPSILON) * input_gain
    ).astype(jnp.bfloat16)
    weight_rows = side_by_side(
        (w_query, w_key, w_value, w_gates, w_glu_value, sigmoid_opener_matrix), "sp", 0, 1
    )
    projected = tuple(
        (
            jnp.dot(normed, rows_here, preferred_element_type=jnp.float32)
            for rows_here in weight_rows
        )
    )
    delta_mix = delta_branch(
        projected[0], projected[1], projected[2], projected[3], log_decay, head_gain
    )
    filtered_blend = conv_branch(projected[4], projected[5], conv_kernel, norm_gain, norm_shift)
    contract = (((1,), (1,)), ((), ()))
    term = lax.dot_general(delta_mix, out_delta, contract, preferred_element_type=jnp.float32)
    term = term + lax.dot_general(
        filtered_blend, out_conv, contract, preferred_element_type=jnp.float32
    )
    return sum_at_owner(term.astype(jnp.bfloat16), "tp", 1).astype(jnp.bfloat16)


def solution(mesh):
    placed = (
        P(("grp", "sp"), None),
        P(),
        P("sp", "tp"),
        P("sp", "tp"),
        P("sp", "tp"),
        P("sp", "tp"),
        P("sp", "tp"),
        P("sp", "tp"),
        P(("grp", "sp"), "tp"),
        P(),
        P(None, "tp"),
        P("tp"),
        P("tp"),
        P(None, "tp"),
        P(None, "tp"),
    )
    return jax.shard_map(
        on_device, mesh=mesh, in_specs=placed, out_specs=P(("grp", "sp"), "tp"), check_vma=False
    )
```

profile of v0, /device:TPU:33, one launch (start us, length us, event | category | flops | bytes accessed | tf_op | source)
XLA Modules:
  0.0 682.0 jit_solution(3263168985769128320)
XLA Ops:
  7.5 1.5 concatenate.9
  9.1 1.5 fusion.93
  11.6 1.0 slice_bitcast_fusion.32
  12.7 1.0 fusion.95
  13.7 139.8 %all-gather.6.cloned.1.call-done = bf16[2048,644]{1,0:T(8,128)(2,1)} async-done(((bf16[64,644]{1,0:T(8,128)(2,1)}), bf16[2048,644]{1,0:T(8,128)(2,1)}) %all-gather.6.cloned.1.call-update) | async-done | bytes 2637840 | tf_op jit(solution)/shard_map/all_gather | solution.py:104
  153.5 1.4 convolution_bitcast_fusion.19
  157.9 1.8 fusion.133
  159.7 1.8 fusion.115
  161.4 1.5 collective-permute-start
  163.0 1.3 collective-permute-start.1
  164.3 1.6 multiply_reduce_fusion.3
  165.9 1.6 multiply_reduce_fusion.2
  168.3 19.7 %custom-call.8 = f32[4,1,64,64]{2,3,1,0:T(8,128)S(1)} custom-call(f32[4,1,64,64]{3,2,1,0:T(8,128)S(1)} %fusion.121), custom_call_target="InvertDiagBlocksLowerTriangular" | custom-call | tf_op jit(solution)/shard_map/jit(_solve_triangular)/vmap()/triangular_solve | solution.py:146
  188.8 19.7 %custom-call.7 = f32[4,1,64,64]{2,3,1,0:T(8,128)S(1)} custom-call(f32[4,1,64,64]{3,2,1,0:T(8,128)S(1)} %fusion.118), custom_call_target="InvertDiagBlocksLowerTriangular" | custom-call | tf_op jit(solution)/shard_map/jit(_solve_triangular)/vmap()/triangular_solve | solution.py:146
  208.8 1.5 divide_multiply_fusion.1
  212.0 14.6 %while.50 = (s32[]{:T(128)}, f32[1,128,128]{2,1,0:T(8,128)S(1)}, f32[1,128,128]{2,1,0:T(8,128)S(1)}, f32[4,1,64,128]{3,2,1,0:T(8,128)S(1)}, f32[4,1,64,128]{3,2,...) while((s32[]{:T(128)}, f32[1,128,128]{2,1,0:T(8,128)S(1)}, ...), condition=%wide.region_5.7_spmd.clone, body=%wide.region_4.6_spmd.clone.sunk | while | flops 100818944 | bytes 1348784 | solution.py:186
  228.5 26.3 %all-to-all-start.2 = ((f32[8,1,512]{2,1,0:T(1,128)}), f32[8,1,512]{2,1,0:T(1,128)S(1)}, u32[]{:S(2)}, u32[]{:S(2)}) async-start(f32[8,1,512]{2,1,0:T(1,128)} %broadcast_in_dim.197), calls=%async_computation.2 | async-start | bytes 32768 | tf_op jit(solution)/shard_map/all_to_all | solution.py:17
  255.2 4.3 all-to-all-done.2
  259.5 1.2 broadcast_in_dim.185
  260.7 15.9 %all-to-all-start = ((bf16[32,1,128,128]{3,2,1,0:T(8,128)(2,1)}), bf16[32,1,128,128]{3,2,1,0:T(8,128)(2,1)S(1)}, u32[]{:S(2)}, u32[]{:S(2)}) async-start(bf16[32,1,128,128]{3,2,1,0:T(8,128)(2,1)} %broadcast_in_dim.185), calls=%async_computation | async-start | bytes 2097152 | tf_op jit(solution)/shard_map/all_to_all | solution.py:17
  276.9 15.2 %while.51 = (s32[]{:T(128)}, f32[1,128,128]{2,1,0:T(8,128)S(1)}, f32[1,128,128]{2,1,0:T(8,128)S(1)}, f32[4,1,64,128]{3,2,1,0:T(8,128)S(1)}, f32[4,1,64,128]{3,2,...) while((s32[]{:T(128)}, f32[1,128,128]{2,1,0:T(8,128)S(1)}, ...), condition=%wide.region_8.10_spmd.clone, body=%wide.region_7.9_spmd.clone.sunk | while | flops 100818944 | bytes 1348784 | solution.py:186
  278.2 1.0 fusion.370
  279.2 1.0 convolution_subtract_fusion.16
  282.0 1.0 fusion.370
  283.0 1.0 convolution_subtract_fusion.16
  285.8 1.0 fusion.370
  286.8 1.0 convolution_subtract_fusion.16
  289.6 1.0 fusion.370
  290.6 1.0 convolution_subtract_fusion.16
  293.7 92.0 %all-to-all-done = bf16[32,1,128,128]{3,2,1,0:T(8,128)(2,1)S(1)} async-done(((bf16[32,1,128,128]{3,2,1,0:T(8,128)(2,1)}), bf16[32,1,128,128]{3,2,1,0:T(8,128)(2,1)S(1)}, u32[]{:S(2)}, u32[]{:S(2)}) %all-to-all-start) | async-done | bytes 1048608 | tf_op jit(solution)/shard_map/all_to_all | solution.py:17
  385.7 1.2 broadcast_in_dim.190
  386.9 7.5 %all-to-all-start.1 = ((bf16[32,1,128,128]{3,2,1,0:T(8,128)(2,1)}), bf16[32,1,128,128]{3,2,1,0:T(8,128)(2,1)S(1)}, u32[]{:S(2)}, u32[]{:S(2)}) async-start(bf16[32,1,128,128]{3,2,1,0:T(8,128)(2,1)} %broadcast_in_dim.190), calls=%async_computation.1 | async-start | bytes 2097152 | tf_op jit(solution)/shard_map/all_to_all | solution.py:17
  395.1 65.3 %all-gather.10.cloned.1.call-done = bf16[32,128,128]{2,1,0:T(8,128)(2,1)} async-done(((bf16[1,128,128]{2,1,0:T(8,128)(2,1)}), bf16[32,128,128]{2,1,0:T(8,128)(2,1)}) %all-gather.10.cloned.1.call-update) | async-done | bytes 1048592 | tf_op jit(solution)/shard_map/all_gather | solution.py:50
  460.5 133.2 %all-gather.8.cloned.1.call-done = bf16[32,128,128]{2,1,0:T(8,128)(2,1)} async-done(((bf16[1,128,128]{2,1,0:T(8,128)(2,1)}), bf16[32,128,128]{2,1,0:T(8,128)(2,1)}) %all-gather.8.cloned.1.call-update) | async-done | bytes 1048592 | tf_op jit(solution)/shard_map/all_gather | solution.py:50
  593.6 32.3 %while.52 = (s32[]{:T(128)}, f32[1,128,128]{2,1,0:T(8,128)S(1)}, s32[]{:T(128)}, bf16[32,1,128,128]{3,2,1,0:T(8,128)(2,1)}, bf16[32,1,128,128]{3,2,1,0:T(8,128)(...) while((s32[]{:T(128)}, f32[1,128,128]{2,1,0:T(8,128)S(1)}, s32[]{:T(128)}, ...), condition=%wide.region_10.12_spmd.clone, body=%wide.region_9.11_spmd.clone.sunk | while | flops 25247752 | bytes 395941 | solution.py:68
  594.6 1.0 fusion.376
  599.7 1.0 fusion.376
  600.7 1.0 fusion.376
  601.7 1.0 fusion.376
  606.8 1.0 fusion.376
  607.8 1.0 fusion.376
  608.8 1.0 fusion.376
  612.9 1.0 fusion.376
  613.9 1.0 fusion.376
  622.0 1.0 fusion.376
  627.1 1.2 convolution_bitcast_fusion.7
  628.4 1.3 fusion.96
  634.0 40.6 %all_to_all.21 = bf16[8,256,256]{2,1,0:T(8,128)(2,1)S(1)} all-to-all(bf16[8,256,256]{2,1,0:T(8,128)(2,1)S(1)} %bitcast.521), channel_id=1, replica_groups=mesh['grp'=2,'sp'=32,'tp'=8] {'tp'}, dimensions={0} | all-to-all | bytes 2097152 | tf_op jit(solution)/shard_map/all_to_all | solution.py:115
  (243 shorter events, 62.1 us)
Async XLA Ops:
  6.5 626.3 %copy-start = (bf16[2048,128]{1,0:T(8,128)(2,1)S(1)}, bf16[2048,128]{1,0:T(8,128)(2,1)}, u32[]{:S(2)}) copy-start(bf16[2048,128]{1,0:T(8,128)(2,1)} %param.36) | copy-start | bytes 1572868
  6.6 6.2 copy-start.4
  6.6 146.9 %all-gather.6.cloned.1.call-start = ((), (), s32[]{:S(2)}) async-start(), calls=%async_computation.4 | async-start | bytes 3244032 | tf_op jit(solution)/shard_map/all_gather | solution.py:104
  9.1 145.8 %copy-start.1 = (f32[1,128,128]{2,1,0:T(8,128)}, f32[1,128,128]{2,1,0:T(8,128)S(1)}, u32[]{:S(2)}) copy-start(f32[1,128,128]{2,1,0:T(8,128)S(1)} %fusion.233) | copy-start | bytes 196612
  10.6 144.3 %copy-start.8 = (f32[256,2]{0,1:T(2,128)S(1)}, f32[256,2]{0,1:T(2,128)}, u32[]{:S(2)}) copy-start(f32[256,2]{0,1:T(2,128)} %param.31) | copy-start | bytes 6148
  161.4 65.8 %collective-permute-start = (bf16[15,128]{1,0:T(8,128)(2,1)S(1)}, bf16[15,128]{1,0:T(8,128)(2,1)S(1)}, u32[]{:S(2)}, u32[]{:S(2)}) collective-permute-start(bf16[15,128]{1,0:T(8,128)(2,1)S(1)} %get-tuple-element.561), channel_id=1, source_target_pairs={{0,8},{8,16},{16,24},{24,32},{32,40},{40,48},{48,56},{56,64},{64,7... | collective-permute-start | bytes 11528 | tf_op jit(solution)/shard_map/ppermute | solution.py:76
  163.0 64.2 %collective-permute-start.1 = (bf16[15,128]{1,0:T(8,128)(2,1)S(1)}, bf16[15,128]{1,0:T(8,128)(2,1)S(1)}, u32[]{:S(2)}, u32[]{:S(2)}) collective-permute-start(bf16[15,128]{1,0:T(8,128)(2,1)S(1)} %get-tuple-element.562), channel_id=1, source_target_pairs={{8,0},{16,8},{24,16},{32,24},{40,32},{48,40},{56,48},{64,56},{72,6... | collective-permute-start | bytes 11528 | tf_op jit(solution)/shard_map/ppermute | solution.py:79
  208.8 3.1 copy-start.3
  226.6 1.3 copy-start.5
  227.8 49.1 %copy-start.2 = (f32[1,128,128]{2,1,0:T(8,128)S(1)}, f32[1,128,128]{2,1,0:T(8,128)}, u32[]{:S(2)}) copy-start(f32[1,128,128]{2,1,0:T(8,128)} %copy-done.1) | copy-start | bytes 196612
  228.5 31.0 %all-to-all-start.2 = ((f32[8,1,512]{2,1,0:T(1,128)}), f32[8,1,512]{2,1,0:T(1,128)S(1)}, u32[]{:S(2)}, u32[]{:S(2)}) async-start(f32[8,1,512]{2,1,0:T(1,128)} %broadcast_in_dim.197), calls=%async_computation.2 | async-start | bytes 32768 | tf_op jit(solution)/shard_map/all_to_all | solution.py:17
  260.7 125.0 %all-to-all-start = ((bf16[32,1,128,128]{3,2,1,0:T(8,128)(2,1)}), bf16[32,1,128,128]{3,2,1,0:T(8,128)(2,1)S(1)}, u32[]{:S(2)}, u32[]{:S(2)}) async-start(bf16[32,1,128,128]{3,2,1,0:T(8,128)(2,1)} %broadcast_in_dim.185), calls=%async_computation | async-start | bytes 2097152 | tf_op jit(solution)/shard_map/all_to_all | solution.py:17
  276.6 183.8 %all-gather.10.cloned.1.call-start = ((), (), s32[]{:S(2)}) async-start(), calls=%async_computation.6 | async-start | bytes 1081344 | tf_op jit(solution)/shard_map/all_gather | solution.py:50
  292.8 300.8 %all-gather.8.cloned.1.call-start = ((), (), s32[]{:S(2)}) async-start(), calls=%async_computation.5 | async-start | bytes 1081344 | tf_op jit(solution)/shard_map/all_gather | solution.py:50
  386.9 239.6 %all-to-all-start.1 = ((bf16[32,1,128,128]{3,2,1,0:T(8,128)(2,1)}), bf16[32,1,128,128]{3,2,1,0:T(8,128)(2,1)S(1)}, u32[]{:S(2)}, u32[]{:S(2)}) async-start(bf16[32,1,128,128]{3,2,1,0:T(8,128)(2,1)} %broadcast_in_dim.190), calls=%async_computation.1 | async-start | bytes 2097152 | tf_op jit(solution)/shard_map/all_to_all | solution.py:17
  395.1 231.4 %copy-start.9 = (pred[32]{0:T(512)(128)(4,1)S(1)}, pred[32]{0:T(512)(128)(4,1)}, u32[]{:S(2)}) copy-start(pred[32]{0:T(512)(128)(4,1)} %iota_compare_fusion.9) | copy-start | bytes 100
  630.3 2.2 copy-start.6
  630.3 2.6 copy-start.10
  631.8 1.7 copy-start.7
  631.8 1.6 copy-start.11
  631.8 1.6 copy-start.12
Sparse Core Ops, SparseCore 0:
  9.4 144.0 all-gather.5
  293.0 167.4 all-gather.9
  462.6 131.0 all-gather.7
where the time goes:
time: 685 us; the launch traced here: 682 us
  waiting for transfers between devices  435 us (64%)
  matrix products  75.1 us (11%)
  starting transfers between devices  52.9 us (8%)
  other arithmetic  47.7 us (7%)
  blocking collectives  40.6 us (6%)
  local copies, waits for them, and re-layouts  15.1 us (2%)
  between operations  13.8 us (2%)
    all_gather x2, waiting for transfers between devices, entering_2(): lax.all_gather(part.astype(kind), axis)  198 us
    all_gather x1, waiting for transfers between devices, side_by_side(): lax.all_gather(both, axis, axis=dim, tiled=True)  140 us
    all_to_all x3, waiting for transfers between devices, from_everyone(): return lax.all_to_all(copies, axis, split_axis=0, concat_axis=0, tiled=True)  96.3 us
    dot_general x114, matrix products, high_dot(): return jnp.matmul(left, right, precision=PRECISE)  63.5 us
    all_to_all x3, starting transfers between devices, from_everyone(): return lax.all_to_all(copies, axis, split_axis=0, concat_axis=0, tiled=True)  49.7 us
    all_to_all x1, blocking collectives, sum_at_owner(): lax.all_to_all(tiles, axis, split_axis=0, concat_axis=0, tiled=True)  40.6 us
    another operation x4, other arithmetic, block_terms(): jax.scipy.linalg.solve_triangular(identity + lower_part, jnp.broadcast_to...  39.4 us
  transfers between devices with their start and end apart: 8, of which 5 were waited for; matrix products, arithmetic and copies ran while one was open for 17% of the time, Pallas kernels for 0%

commit v1 on v0

v1 whole, which is shorter than its diff:
```python
import functools

import jax
import jax.numpy as jnp
from jax import lax
from jax.experimental import pallas as pl
from jax.experimental.pallas import tpu as pltpu
from jax.sharding import PartitionSpec as P

EPSILON = 1e-06
BETA_SHIFT = 6.0
SPAN = 4
PARTS = 2
MESH = pl.DeviceIdType.MESH
F32 = jnp.float32
BF16 = jnp.bfloat16


def dot(a, b, dims=((1,), (0,))):
    return lax.dot_general(a, b, (dims, ((), ())), preferred_element_type=F32)


def bf_dot(a, b, dims=((1,), (0,))):
    return dot(a.astype(BF16), b.astype(BF16), dims)


def split(a):
    high = a.astype(BF16)
    return high, (a - high.astype(F32)).astype(BF16)


def fine_dot(a, b, dims=((1,), (0,))):
    ah, al = split(a)
    bh, bl = split(b)
    return dot(ah, bh, dims) + (dot(al, bh, dims) + dot(ah, bl, dims))


def mask_dot(mask, b):
    high, rest = split(b)
    middle = b - high.astype(F32) - rest.astype(F32)
    return dot(mask, high) + (dot(mask, rest) + dot(mask, middle.astype(BF16)))


def sigmoid(a):
    return 1.0 / (1.0 + jnp.exp(-a))


def silu(a):
    return a * sigmoid(a)


def unit_rows(a):
    return a * lax.rsqrt(jnp.sum(a * a, axis=-1, keepdims=True) + EPSILON)


def unit_inverse(a):
    size = a.shape[0]
    row = lax.broadcasted_iota(jnp.int32, (size, size), 0)
    col = lax.broadcasted_iota(jnp.int32, (size, size), 1)
    apart = row ^ col
    inverse = jnp.where(row == col, 1.0, jnp.where(apart < 2, -a, 0.0))
    half = 2
    while half < size:
        corner = jnp.where((apart >= half) & (apart < 2 * half), a, 0.0)
        inverse = inverse - fine_dot(inverse, fine_dot(corner, inverse))
        half *= 2
    return inverse


def triangular_inverse(a, upper):
    half = a.shape[0] // 2
    first = unit_inverse(a[:half, :half])
    second = unit_inverse(a[half:, half:])
    zero = jnp.zeros((half, half), F32)
    if upper:
        corner = -fine_dot(first, fine_dot(a[:half, half:], second))
        rows = (jnp.concatenate([first, corner], 1), jnp.concatenate([zero, second], 1))
    else:
        corner = -fine_dot(second, fine_dot(a[half:, :half], first))
        rows = (jnp.concatenate([first, zero], 1), jnp.concatenate([corner, second], 1))
    return jnp.concatenate(rows, 0)


def delta_block(query, key_rows, values, keys_keys, query_keys, total_col, total_row, beta, upper):
    length, width = key_rows.shape
    row = lax.broadcasted_iota(jnp.int32, (length, length), 0)
    col = lax.broadcasted_iota(jnp.int32, (length, length), 1)
    within = (col >= row) if upper else (row >= col)
    weighting = jnp.where(within, jnp.exp(jnp.minimum(total_col - total_row, 0.0)), 0.0)
    coupling = jnp.where(row == col, 0.0, beta * keys_keys * weighting)
    inverse = triangular_inverse(coupling, upper)
    decayed = jnp.exp(total_col)
    sources = jnp.concatenate([beta * values, (beta * decayed) * key_rows], 1)
    sources = bf_dot(inverse, sources).astype(BF16)
    here = bf_dot(query_keys * weighting, sources)
    end = total_col[0:1, :] if upper else total_col[length - 1 :, :]
    leaving = key_rows * jnp.exp(end - total_col)
    update = bf_dot(leaving, sources, ((0,), (0,)))
    eye = jnp.where(
        lax.broadcasted_iota(jnp.int32, (width, width), 0)
        == lax.broadcasted_iota(jnp.int32, (width, width), 1),
        1.0,
        0.0,
    )
    state_map = jnp.exp(end) * eye - update[:, width:]
    reading = query * decayed - here[:, width:]
    return here[:, :width], reading, jnp.concatenate([state_map, update[:, :width]], 1)


def layer_kernel(
    nz,
    nt,
    x_ref,
    gain_ref,
    wq_ref,
    wk_ref,
    wv_ref,
    wg_ref,
    wc_ref,
    ws_ref,
    decay_ref,
    head_gain_ref,
    taps_ref,
    norm_gain_ref,
    norm_shift_ref,
    od_ref,
    oc_ref,
    out_ref,
    w_buf,
    g_buf,
    od_buf,
    oc_buf,
    fd_buf,
    fc_buf,
    stat_buf,
    normed_ref,
    proj_ref,
    glu_ref,
    halo_ref,
    pad_ref,
    square_ref,
    local_ref,
    read_ref,
    own_ref,
    near_ref,
    prefix_ref,
    head_ref,
    far_ref,
    state_ref,
    enter_send,
    enter_ref,
    load_sem,
    ring_send,
    ring_recv,
    gate_send,
    gate_recv,
    out_send,
    out_recv,
    halo_send,
    halo_recv,
    stat_send,
    stat_recv,
    fc_send,
    fc_recv,
    fd_send,
    fd_recv,
    near_send,
    near_recv,
    far_send,
    far_recv,
    enter_send_sem,
    enter_recv,
):
    z = lax.axis_index("sp")
    t = lax.axis_index("tp")
    rows = wq_ref.shape[0]
    length = x_ref.shape[0]
    width = wq_ref.shape[1]
    out_cols = out_ref.shape[1]
    piece = rows // PARTS
    blocks = nz // SPAN
    right = lax.rem(z + 1, nz)
    left = lax.rem(z + nz - 1, nz)
    ups = nz // 2
    downs = nz - 1 - ups

    def to(zz, tt):
        return {"sp": zz, "tp": tt}

    def remote(src, dst, send, recv, where):
        return pltpu.make_async_remote_copy(
            src_ref=src,
            dst_ref=dst,
            send_sem=send,
            recv_sem=recv,
            device_id=where,
            device_id_type=MESH,
        )

    def lane_block(index):
        return pl.ds(pl.multiple_of(index * width, width), width)

    loads = []
    base = pl.multiple_of(z * rows, rows)
    for n, src in enumerate((wk_ref, wv_ref, wq_ref, wc_ref, ws_ref)):
        loads.append(
            pltpu.make_async_copy(
                src,
                w_buf.at[pl.ds(base, rows), pl.ds(n * width, width)],
                load_sem.at[n],
            )
        )
    loads.append(pltpu.make_async_copy(od_ref.at[pl.ds(pl.multiple_of(t * out_cols, out_cols), out_cols), :], od_buf.at[:, lane_block(t)], load_sem.at[5]))
    loads.append(pltpu.make_async_copy(oc_ref.at[pl.ds(pl.multiple_of(t * out_cols, out_cols), out_cols), :], oc_buf.at[:, lane_block(t)], load_sem.at[6]))
    for load in loads:
        load.start()

    square_ref[...] = jnp.zeros_like(square_ref)
    square_ref[0:rows, 0:4] = wg_ref[...].astype(F32)
    flat = jnp.transpose(square_ref[0:width, :])[0:16, :]
    if 2 * rows == width:
        odd = lax.rem(z, 2) == 1
        flat = jnp.where(odd, pltpu.roll(flat, rows, 1), flat)
    g_buf[z] = flat.astype(BF16)

    barrier = pltpu.get_barrier_semaphore()
    pl.semaphore_signal(barrier, inc=1, device_id=to(right, t), device_id_type=MESH)
    pl.semaphore_signal(barrier, inc=1, device_id=to(left, t), device_id_type=MESH)
    for d in range(1, nt):
        pl.semaphore_signal(
            barrier, inc=1, device_id=to(z, lax.rem(t + d, nt)), device_id_type=MESH
        )
    pl.semaphore_wait(barrier, nt + 1)
    for load in loads:
        load.wait()

    def chunk_copy(origin, part, way, step):
        at = pl.ds(pl.multiple_of(origin * rows + part * piece, piece), piece)
        return remote(
            w_buf.at[at, :],
            w_buf.at[at, :],
            ring_send.at[way, step, part],
            ring_recv.at[way, step, part],
            to((right, left)[way], t),
        )

    def gate_copy(origin, way, step):
        return remote(
            g_buf.at[origin],
            g_buf.at[origin],
            gate_send.at[way, step],
            gate_recv.at[way, step],
            to((right, left)[way], t),
        )

    for part in range(PARTS):
        chunk_copy(z, part, 0, 0).start()
        chunk_copy(z, part, 1, 0).start()
    gate_copy(z, 0, 0).start()
    gate_copy(z, 1, 0).start()

    def out_copy(d):
        owner = lax.rem(t + d, nt)
        block = pl.ds(pl.multiple_of(owner * out_cols, out_cols), out_cols)
        return (
            remote(od_ref.at[block, :], od_buf.at[:, lane_block(t)], out_send.at[0, d - 1], out_recv.at[0, d - 1], to(z, owner)),
            remote(oc_ref.at[block, :], oc_buf.at[:, lane_block(t)], out_send.at[1, d - 1], out_recv.at[1, d - 1], to(z, owner)),
        )

    for d in range(1, nt):
        for copy in out_copy(d):
            copy.start()

    x = x_ref[...].astype(F32)
    scale = lax.rsqrt(jnp.mean(x * x, axis=-1, keepdims=True) + EPSILON)
    normed_ref[...] = (x * scale * gain_ref[...]).astype(BF16)

    def ring_step(step, carry):
        up = lax.rem(z + nz - step, nz)
        down = lax.rem(z + step, nz)
        for part in range(PARTS):
            chunk_copy(up, part, 0, step - 1).wait_recv()
            chunk_copy(up, part, 0, step).start()
            chunk_copy(down, part, 1, step - 1).wait_recv()

            @pl.when(step < downs)
            def _():
                chunk_copy(down, part, 1, step).start()

        gate_copy(up, 0, step - 1).wait_recv()
        gate_copy(up, 0, step).start()
        gate_copy(down, 1, step - 1).wait_recv()

        @pl.when(step < downs)
        def _():
            gate_copy(down, 1, step).start()

        return carry

    lax.fori_loop(1, ups, ring_step, 0)
    last = lax.rem(z + nz - ups, nz)
    for part in range(PARTS):
        chunk_copy(last, part, 0, ups - 1).wait_recv()
    gate_copy(last, 0, ups - 1).wait_recv()

    normed = normed_ref[...]
    proj_ref[...] = dot(normed, w_buf[...])
    gate_rows = jnp.concatenate(
        [
            g_buf[2 * m] + g_buf[2 * m + 1] if 2 * rows == width else g_buf[m]
            for m in range(nz * rows // width)
        ],
        1,
    )
    gates = dot(normed, gate_rows, ((1,), (1,)))

    glu = (proj_ref[:, 3 * width : 4 * width] * sigmoid(proj_ref[:, 4 * width :])).astype(BF16)
    glu_ref[...] = glu
    edge = halo_ref.shape[1]
    edge_up = remote(glu_ref.at[pl.ds(length - edge, edge), :], halo_ref.at[0], halo_send.at[0], halo_recv.at[0], to(right, t))
    edge_down = remote(glu_ref.at[pl.ds(0, edge), :], halo_ref.at[1], halo_send.at[1], halo_recv.at[1], to(left, t))
    edge_up.start()
    edge_down.start()

    key_rows = unit_rows(silu(proj_ref[:, 0:width]))
    values = silu(proj_ref[:, width : 2 * width])
    query = unit_rows(silu(proj_ref[:, 2 * width : 3 * width])) * width ** (-0.5)
    lane = lax.broadcasted_iota(jnp.int32, gates.shape, 1)
    shift = jnp.where((lane == 1) | (lane == 3), BETA_SHIFT, 0.0)
    opened = sigmoid(gates - shift)
    base_decay = jnp.where(
        lane == 0, decay_ref[:, 0:1], jnp.where(lane == 2, decay_ref[:, 1:2], 0.0)
    )
    decays = base_decay * (0.5 + opened)
    row = lax.broadcasted_iota(jnp.int32, (length, length), 0)
    col = lax.broadcasted_iota(jnp.int32, (length, length), 1)
    below = jnp.where(row >= col, 1.0, 0.0).astype(BF16)
    above = jnp.where(col >= row, 1.0, 0.0).astype(BF16)
    totals = jnp.where(lane == 0, mask_dot(below, decays), mask_dot(above, decays))
    square_ref[:, 0 : gates.shape[1]] = totals
    total_rows = jnp.transpose(square_ref[...])
    keys_keys = fine_dot(key_rows, key_rows, ((1,), (1,)))
    query_keys = bf_dot(query, key_rows, ((1,), (1,)))
    here = []
    for way in (0, 1):
        output, reading, affine = delta_block(
            query,
            key_rows,
            values,
            keys_keys,
            query_keys,
            totals[:, 2 * way : 2 * way + 1],
            total_rows[2 * way : 2 * way + 1, :],
            opened[:, 2 * way + 1 : 2 * way + 2],
            way == 1,
        )
        here.append(output)
        read_ref[way] = reading.astype(BF16)
        own_ref[way] = affine.astype(BF16)
    local_ref[...] = here[0] + here[1]

    place = lax.rem(z, SPAN)
    block = z // SPAN
    near = []
    for d in range(SPAN - 1, 0, -1):
        for way in (0, 1):
            fits = (place + d < SPAN) if way == 0 else (place >= d)
            target = lax.rem(z + (d if way == 0 else nz - d), nz)
            copy = remote(own_ref.at[way], near_ref.at[way, place], near_send.at[way, d - 1], near_recv.at[way, d - 1], to(target, t))
            near.append((fits, copy))

            @pl.when(fits)
            def _():
                copy.start()

    edge_up.wait_recv()
    edge_down.wait_recv()
    taps = taps_ref.shape[0]
    half_width = taps // 2
    pad_ref[0:edge, :] = jnp.where(z == 0, 0.0, halo_ref[0].astype(F32))
    pad_ref[edge : edge + length, :] = glu_ref[...].astype(F32)
    pad_ref[edge + length :, :] = jnp.where(z == nz - 1, 0.0, halo_ref[1].astype(F32))
    start = edge - half_width
    conv = pad_ref[start : start + length, :] * taps_ref[0:1, :]
    for offset in range(1, taps):
        conv = conv + pad_ref[start + offset : start + offset + length, :] * taps_ref[offset : offset + 1, :]
    square_ref[:, 0:1] = jnp.sum(conv, axis=-1, keepdims=True)
    square_ref[:, 1:2] = jnp.sum(conv * conv, axis=-1, keepdims=True)
    stat_buf[t] = jnp.transpose(square_ref[...])[0:8, :]

    def stat_copy(d):
        return remote(stat_buf.at[t], stat_buf.at[t], stat_send.at[d - 1], stat_recv.at[d - 1], to(z, lax.rem(t + d, nt)))

    for d in range(1, nt):
        stat_copy(d).start()
    proj_ref[:, 0:width] = conv

    for way in (0, 1):
        eye = jnp.where(
            lax.broadcasted_iota(jnp.int32, (width, 2 * width), 0)
            == lax.broadcasted_iota(jnp.int32, (width, 2 * width), 1),
            1.0,
            0.0,
        )
        prefix_ref[way] = eye
    right_part = lax.broadcasted_iota(jnp.int32, (width, 2 * width), 1) >= width

    def compose(affine, before):
        return bf_dot(affine[:, 0:width], before) + jnp.where(right_part, affine.astype(F32), 0.0)

    for step in range(SPAN - 1):
        for way in (0, 1):
            origin = step if way == 0 else SPAN - 1 - step
            comes = (place > origin) if way == 0 else (place < origin)
            distance = (place - origin) if way == 0 else (origin - place)

            @pl.when(comes)
            def _():
                remote(
                    own_ref.at[way],
                    near_ref.at[way, origin],
                    near_send.at[way, 0],
                    near_recv.at[way, distance - 1],
                    to(right, t),
                ).wait_recv()
                prefix_ref[way] = compose(near_ref[way, origin], prefix_ref[way])

    def leads(way):
        if way == 0:
            return (place == SPAN - 1) & (block < blocks - 1)
        return (place == 0) & (block > 0)

    def far_copy(way, d):
        target = lax.rem(z + (SPAN * d if way == 0 else nz - SPAN * d), nz)
        return remote(head_ref.at[way], far_ref.at[way, block], far_send.at[way, d - 1], far_recv.at[way, d - 1], to(target, t))

    def far_fits(way, d):
        if way == 0:
            return leads(way) & (block + d < blocks - 1)
        return leads(way) & (block - d > 0)

    for way in (0, 1):

        @pl.when(leads(way))
        def _():
            head_ref[way] = compose(own_ref[way], prefix_ref[way]).astype(BF16)

    for d in range(blocks - 2, 0, -1):
        for way in (0, 1):

            @pl.when(far_fits(way, d))
            def _():
                far_copy(way, d).start()

    total = stat_buf[t]
    for d in range(1, nt):
        stat_copy(d).wait_recv()
    for d in range(1, nt):
        total = total + stat_buf[lax.rem(t + nt - d, nt)]
    square_ref[0:width, :] = jnp.zeros((width, width), F32)
    stats = jnp.transpose(jnp.concatenate([total, jnp.zeros((width - 8, length), F32)], 0))
    channels = nt * width
    center = stats[:, 0:1] / channels
    spread = stats[:, 1:2] / channels - center * center
    normal = (proj_ref[:, 0:width] - center) * lax.rsqrt(spread + EPSILON)
    fc_buf[:, lane_block(t)] = silu(normal * norm_gain_ref[...] + norm_shift_ref[...]).astype(BF16)

    def feature_copy(buf, send, recv, d):
        return remote(buf.at[:, lane_block(t)], buf.at[:, lane_block(t)], send.at[d - 1], recv.at[d - 1], to(z, lax.rem(t + d, nt)))

    for d in range(1, nt):
        feature_copy(fc_buf, fc_send, fc_recv, d).start()

    for way in (0, 1):

        @pl.when(leads(way))
        def _():
            state_ref[way] = jnp.zeros((width, width), F32)

    for step in range(blocks - 2):
        for way in (0, 1):
            origin = step if way == 0 else blocks - 1 - step
            comes = leads(way) & ((block > origin) if way == 0 else (block < origin))
            distance = (block - origin) if way == 0 else (origin - block)

            @pl.when(comes)
            def _():
                remote(
                    head_ref.at[way],
                    far_ref.at[way, origin],
                    far_send.at[way, 0],
                    far_recv.at[way, distance - 1],
                    to(right, t),
                ).wait_recv()
                affine = far_ref[way, origin]
                state_ref[way] = bf_dot(affine[:, 0:width], state_ref[way]) + affine[:, width:].astype(F32)

    def enter_copy(way, d):
        target = lax.rem(z + (d if way == 0 else nz - d), nz)
        slot = (d - 1) if way == 0 else (SPAN - d)
        return remote(enter_send.at[way], enter_ref.at[way], enter_send_sem.at[way, d - 1], enter_recv.at[way], to(target, t))

    for way in (0, 1):

        @pl.when(leads(way))
        def _():
            affine = head_ref[way]
            state = bf_dot(affine[:, 0:width], state_ref[way]) + affine[:, width:].astype(F32)
            enter_send[way] = state.astype(BF16)
            for d in range(SPAN, 0, -1):
                enter_copy(way, d).start()

    for d in range(1, nt):
        for copy in out_copy(d):
            copy.wait_recv()
        feature_copy(fc_buf, fc_send, fc_recv, d).wait_recv()
    mixed = dot(fc_buf[...], oc_buf[...], ((1,), (1,)))

    for way in (0, 1):
        state_ref[way] = prefix_ref[way][:, width:]
        follows = (block > 0) if way == 0 else (block < blocks - 1)

        @pl.when(follows)
        def _():
            enter_copy(way, 1).wait_recv()
            state_ref[way] = state_ref[way] + bf_dot(prefix_ref[way][:, 0:width], enter_ref[way])

    joined = local_ref[...]
    for way in (0, 1):
        joined = joined + bf_dot(read_ref[way], state_ref[way])
    joined = joined * lax.rsqrt(jnp.mean(joined * joined, axis=-1, keepdims=True) + EPSILON)
    fd_buf[:, lane_block(t)] = (joined * head_gain_ref[...]).astype(BF16)
    for d in range(1, nt):
        feature_copy(fd_buf, fd_send, fd_recv, d).start()
    for d in range(1, nt):
        feature_copy(fd_buf, fd_send, fd_recv, d).wait_recv()
    out_ref[...] = (mixed + dot(fd_buf[...], od_buf[...], ((1,), (1,)))).astype(BF16)

    def drain(step, carry):
        for part in range(PARTS):
            chunk_copy(z, part, 0, step).wait_send()
        gate_copy(z, 0, step).wait_send()

        @pl.when(step < downs)
        def _():
            for part in range(PARTS):
                chunk_copy(z, part, 1, step).wait_send()
            gate_copy(z, 1, step).wait_send()

        return carry

    lax.fori_loop(0, ups, drain, 0)
    edge_up.wait_send()
    edge_down.wait_send()
    for d in range(1, nt):
        for copy in out_copy(d):
            copy.wait_send()
        stat_copy(d).wait_send()
        feature_copy(fc_buf, fc_send, fc_recv, d).wait_send()
        feature_copy(fd_buf, fd_send, fd_recv, d).wait_send()
    for fits, copy in near:

        @pl.when(fits)
        def _():
            copy.wait_send()

    for way in (0, 1):
        for d in range(blocks - 2, 0, -1):

            @pl.when(far_fits(way, d))
            def _():
                far_copy(way, d).wait_send()

        @pl.when(leads(way))
        def _():
            for d in range(SPAN, 0, -1):
                enter_copy(way, d).wait_send()


def on_device(
    nz,
    nt,
    tokens_in,
    input_gain,
    w_query,
    w_key,
    w_value,
    w_gates,
    w_glu_value,
    sigmoid_opener_matrix,
    log_decay,
    head_gain,
    conv_kernel,
    norm_gain,
    norm_shift,
    out_delta,
    out_conv,
):
    length, features = tokens_in.shape
    rows, width = w_query.shape
    out_cols = out_delta.shape[0] // nt
    blocks = nz // SPAN
    ups = nz // 2
    edge = 16
    vmem = pl.BlockSpec(memory_space=pltpu.VMEM)
    hbm = pl.BlockSpec(memory_space=pl.ANY)
    dma = pltpu.SemaphoreType.DMA
    scratch = [
        pltpu.VMEM((nz * rows, 5 * width), BF16),
        pltpu.VMEM((nz, 16, width), BF16),
        pltpu.VMEM((out_cols, nt * width), BF16),
        pltpu.VMEM((out_cols, nt * width), BF16),
        pltpu.VMEM((length, nt * width), BF16),
        pltpu.VMEM((length, nt * width), BF16),
        pltpu.VMEM((nt, 8, length), F32),
        pltpu.VMEM((length, features), BF16),
        pltpu.VMEM((length, 5 * width), F32),
        pltpu.VMEM((length, width), BF16),
        pltpu.VMEM((2, edge, width), BF16),
        pltpu.VMEM((length + 2 * edge, width), F32),
        pltpu.VMEM((length, width), F32),
        pltpu.VMEM((length, width), F32),
        pltpu.VMEM((2, length, width), BF16),
        pltpu.VMEM((2, width, 2 * width), BF16),
        pltpu.VMEM((2, SPAN, width, 2 * width), BF16),
        pltpu.VMEM((2, width, 2 * width), F32),
        pltpu.VMEM((2, width, 2 * width), BF16),
        pltpu.VMEM((2, blocks, width, 2 * width), BF16),
        pltpu.VMEM((2, width, width), F32),
        pltpu.VMEM((2, width, width), BF16),
        pltpu.VMEM((2, width, width), BF16),
        dma((7,)),
        dma((2, ups, PARTS)),
        dma((2, ups, PARTS)),
        dma((2, ups)),
        dma((2, ups)),
        dma((2, nt - 1)),
        dma((2, nt - 1)),
        dma((2,)),
        dma((2,)),
        dma((nt - 1,)),
        dma((nt - 1,)),
        dma((nt - 1,)),
        dma((nt - 1,)),
        dma((nt - 1,)),
        dma((nt - 1,)),
        dma((2, SPAN - 1)),
        dma((2, SPAN - 1)),
        dma((2, max(blocks - 2, 1))),
        dma((2, max(blocks - 2, 1))),
        dma((2, SPAN)),
        dma((2,)),
    ]
    return pl.pallas_call(
        functools.partial(layer_kernel, nz, nt),
        name="layer",
        out_shape=jax.ShapeDtypeStruct((length, out_cols), BF16),
        in_specs=[vmem, vmem, hbm, hbm, hbm, vmem, hbm, hbm, vmem, vmem, vmem, vmem, vmem, hbm, hbm],
        out_specs=vmem,
        scratch_shapes=scratch,
        compiler_params=pltpu.CompilerParams(
            collective_id=0, has_side_effects=True, vmem_limit_bytes=48 * 1024 * 1024
        ),
    )(
        tokens_in,
        input_gain.reshape(1, -1),
        w_query,
        w_key,
        w_value,
        w_gates,
        w_glu_value,
        sigmoid_opener_matrix,
        log_decay,
        head_gain.reshape(1, -1),
        conv_kernel,
        norm_gain.reshape(1, -1),
        norm_shift.reshape(1, -1),
        out_delta,
        out_conv,
    )


def solution(mesh):
    placed = (
        P(("grp", "sp"), None),
        P(),
        P("sp", "tp"),
        P("sp", "tp"),
        P("sp", "tp"),
        P("sp", "tp"),
        P("sp", "tp"),
        P("sp", "tp"),
        P(("grp", "sp"), "tp"),
        P(),
        P(None, "tp"),
        P("tp"),
        P("tp"),
        P(None, "tp"),
        P(None, "tp"),
    )
    return jax.shard_map(
        functools.partial(on_device, mesh.shape["sp"], mesh.shape["tp"]),
        mesh=mesh,
        in_specs=placed,
        out_specs=P(("grp", "sp"), "tp"),
        check_vma=False,
    )
```

time: 685 us -> 154 us (0.22)
  waiting for transfers between devices: 435 us -> 0 us
  Pallas kernels: 0 us -> 147 us
  matrix products: 75.1 us -> 0 us
  starting transfers between devices: 52.9 us -> 0 us
  other arithmetic: 47.7 us -> 0 us
  blocking collectives: 40.6 us -> 0 us
  between operations: 13.8 us -> 0.09 us
  local copies, waits for them, and re-layouts: 15.1 us -> 6.07 us
    all_gather x3 -> x0, waiting for transfers between devices: 338 us -> none  [the longest x2 198 us: entering_2(): lax.all_gather(part.astype(kind), axis)]
    pallas_call x0 -> x1, Pallas kernels: none -> 147 us  [on_device(): pl.pallas_call(functools.partial(layer_kernel, nz, nt), name='layer', out...]
    all_to_all x3 -> x0, waiting for transfers between devices: 96.3 us -> none  [from_everyone(): return lax.all_to_all(copies, axis, split_axis=0, concat_axis=0, tiled=True)]
    dot_general x122 -> x0, matrix products: 74.1 us -> none  [the longest x114 63.5 us: high_dot(): return jnp.matmul(left, right, precision=PRECISE)]
    all_to_all x3 -> x0, starting transfers between devices: 49.7 us -> none  [from_everyone(): return lax.all_to_all(copies, axis, split_axis=0, concat_axis=0, tiled=True)]
    all_to_all x1 -> x0, blocking collectives: 40.6 us -> none  [sum_at_owner(): lax.all_to_all(tiles, axis, split_axis=0, concat_axis=0, tiled=True)]
    another operation x6 -> x0, other arithmetic: 39.9 us -> none  [the longest x4 39.4 us: block_terms(): jax.scipy.linalg.solve_triangular(identity + lower_part, jnp.broadcast_to...]
  transfers between devices with their start and end apart: 8 -> 0, of which waited for: 5 -> 0; matrix products, arithmetic and copies ran while one was open for 17% -> 0% of each run, Pallas kernels for 0% -> 0%
where the time goes in v1:
time: 154 us
  Pallas kernels  147 us (95%)
  local copies, waits for them, and re-layouts  6.07 us (4%)
    pallas_call x1, Pallas kernels, on_device(): pl.pallas_call(functools.partial(layer_kernel, nz, nt), name='layer', out...  147 us
    unnamed x33, local copies, waits for them, and re-layouts  6.07 us

profile of v1, /device:TPU:33, one launch (start us, length us, event | category | flops | bytes accessed | tf_op | source)
XLA Modules:
  0.0 153.5 jit_solution(9611097412478745234)
XLA Ops:
  0.0 0.0 copy-start.14
  0.0 0.7 copy-done.14
  0.7 0.0 copy-start.13
  0.7 0.1 copy.16.wg_ref
  0.8 0.6 copy-done.13
  1.4 0.0 copy-start.3
  1.4 0.0 copy-start.4
  1.4 0.0 copy-start.5
  1.4 0.0 copy-start.6
  1.4 0.0 copy-start.7
  1.4 0.0 copy-start.8
  1.4 0.0 copy-start.9
  1.4 0.0 copy-start.10
  1.4 0.0 copy-start.11
  1.4 0.0 copy-start.12
  1.4 0.1 copy.17.decay_ref
  1.6 0.5 copy-done.3
  2.1 0.0 copy-done.4
  2.1 0.0 copy-done.5
  2.1 0.0 copy-done.6
  2.1 0.0 copy-done.7
  2.1 0.0 copy-done.8
  2.2 0.0 copy-done.9
  2.2 0.0 copy-done.10
  2.2 0.0 copy-done.11
  2.2 0.0 copy-done.12
  2.2 0.0 copy-start
  2.2 1.2 copy-done
  3.4 0.0 copy-start.1
  3.4 1.0 copy-done.1
  4.4 0.0 copy-start.2
  4.4 1.0 copy-done.2
  5.5 147.4 %layer.1 = bf16[256,256]{1,0:T(8,128)(2,1)S(1)} custom-call(bf16[256,2048]{1,0:T(8,128)(2,1)S(1)} %copy-done, f32[1,2048]{1,0:T(1,128)S(1)} %bitcast.4, bf16[64,128]{1,0:T(8,128)(2,1)S(1)} %copy-done.3, bf16[64,128]{1,0:T(8,128)(2,1)S(1)} %copy-done.4, bf16[64,128]{1,0:T(8,128)(2,1)S(1)} %copy-done.5, bf16[64,4]{1,0:T(8,128)(2,1)S(1)} %copy.16.wg_ref, ...), custom_call_target="tpu_custom_call" | custom-call | tf_op jit(solution)/shard_map/layer/pallas_call | solution.py:654
  152.9 0.7 copy.19
Async XLA Ops:
  0.0 0.7 copy-start.14
  0.7 0.7 copy-start.13
  1.4 0.7 copy-start.3
  1.4 0.7 copy-start.4
  1.4 0.7 copy-start.5
  1.4 0.8 copy-start.6
  1.4 0.8 copy-start.7
  1.4 0.8 copy-start.8
  1.4 0.8 copy-start.9
  1.4 0.8 copy-start.10
  1.4 0.7 copy-start.11
  1.4 0.7 copy-start.12
  2.2 1.2 copy-start
  3.4 1.0 copy-start.1
  4.4 1.0 copy-start.2
